TPU v7x, 32 devices: a whole 2x2x4 slice. The times are simulated.
32 devices in a mesh: sp: 16 (over z, y, x), dp: 2 (over core).
Axes of the slice: x: 2, y: 2, z: 4, core: 2. Of those that a mesh axis runs over, the one named last changes fastest.
Arguments:
- tokens: bfloat16 [2048, 2048], P('sp', 'dp'), may hold values from -6 to 6
- cotangent: bfloat16 [2048, 2048], P('sp', 'dp'), may hold values from -6 to 6
- in_weight: bfloat16 [256, 2048], P('sp', 'dp'), may hold values from -0.125 to 0.125
- out_weight: bfloat16 [256, 2048], P('sp', 'dp'), may hold values from -0.375 to 0.375
- decay_rate: float32 [16, 32], P('sp'), may hold values from 0 to 1
- frequency: float32 [16, 32], P('sp'), may hold values from 4 to 40
- step_log: float32 [16], P('sp'), may hold values from -2.6593 to -1.9661
- drive_real: float32 [16, 32, 16], P('sp'), may hold values from -6 to 6
- drive_imag: float32 [16, 32, 16], P('sp'), may hold values from -6 to 6
- readout_real_part: float32 [16, 16, 32], P('sp'), may hold values from -0.75 to 0.75
- readout_imaginary: float32 [16, 16, 32], P('sp'), may hold values from -0.75 to 0.75
- skip_gain: float32 [16, 16], P('sp'), may hold values from -4 to 4
Outputs:
- grad_tokens: bfloat16 [2048, 2048], P('sp', 'dp')
- grad_in_weight: float32 [256, 2048], P('sp', 'dp')
- grad_out_weight: float32 [256, 2048], P('sp', 'dp')
All inputs are finite; a program needn't handle non-finite values.
Results may differ from a plain program's by a relative error of at most 0.02.
Values may be sent and summed in bfloat16 or wider, within the bound.
A program may use at most 64 MiB of HBM per device.

v0:
```python
import jax
import jax.numpy as jnp
from jax import lax
from jax.sharding import PartitionSpec as P

finest_precision = lax.Precision.HIGHEST


def combine(earlier, later):
    first_real, first_imag, first_sum_real, first_sum_imag = earlier
    next_real, next_imag, next_sum_real, next_sum_imag = later
    return (
        first_real * next_real - first_imag * next_imag,
        first_real * next_imag + first_imag * next_real,
        next_real * first_sum_real - next_imag * first_sum_imag + next_sum_real,
        next_real * first_sum_imag + next_imag * first_sum_real + next_sum_imag,
    )


def discretize(decay_rate, frequency, step_log, drive_real, drive_imag):
    step_size = jnp.exp(step_log)[..., None]
    magnitude = jnp.exp(-decay_rate * step_size)
    angle = frequency * step_size
    decay_real = magnitude * jnp.cos(angle)
    decay_imag = magnitude * jnp.sin(angle)
    modulus = decay_rate * decay_rate + frequency * frequency
    hold_real = (-decay_rate * (decay_real - 1.0) + frequency * decay_imag) / modulus
    hold_imag = (-frequency * (decay_real - 1.0) - decay_rate * decay_imag) / modulus
    input_real = hold_real[..., None] * drive_real - hold_imag[..., None] * drive_imag
    input_imag = hold_real[..., None] * drive_imag + hold_imag[..., None] * drive_real
    return (decay_real, decay_imag, input_real, input_imag)


def mechanism(head_drive, head_back, params):
    (
        decay_rate,
        frequency,
        step_log,
        drive_real,
        drive_imag,
        readout_real_part,
        readout_imaginary,
        skip_gain,
    ) = params
    group_count, states = decay_rate.shape
    own_width, length = head_drive.shape
    per_group = own_width // group_count
    block_len = min(512, length)
    blocks_total = length // block_len
    decay_real, decay_imag, input_real, input_imag = discretize(
        decay_rate, frequency, step_log, drive_real, drive_imag
    )
    factor_real = jnp.broadcast_to(decay_real[:, :, None], (group_count, states, block_len))
    factor_imag = jnp.broadcast_to(decay_imag[:, :, None], (group_count, states, block_len))

    def to_blocks(matrix):
        shaped = matrix.astype(jnp.float32).reshape(group_count, per_group, blocks_total, block_len)
        return jnp.moveaxis(shaped, 2, 0)

    def forward(carried, drive_block):
        state_real, state_imag = carried
        push_real = jnp.einsum("gpc,gck->gpk", input_real, drive_block, precision=finest_precision)
        push_imag = jnp.einsum("gpc,gck->gpk", input_imag, drive_block, precision=finest_precision)
        push_real = push_real.at[:, :, 0].add(decay_real * state_real - decay_imag * state_imag)
        push_imag = push_imag.at[:, :, 0].add(decay_real * state_imag + decay_imag * state_real)
        _, _, running_real_part, running_imaginary = lax.associative_scan(
            combine, (factor_real, factor_imag, push_real, push_imag), axis=2
        )
        mixed_rows = (
            jnp.einsum(
                "mow,mwn->mon", readout_real_part, running_real_part, precision=finest_precision
            )
            - jnp.einsum(
                "mow,mwn->mon", readout_imaginary, running_imaginary, precision=finest_precision
            )
            + skip_gain[:, :, None] * drive_block
        )
        return ((running_real_part[:, :, -1], running_imaginary[:, :, -1]), mixed_rows)

    empty_state = jnp.zeros((group_count, states), jnp.float32)
    _, mixed_blocks = lax.scan(forward, (empty_state, empty_state), to_blocks(head_drive))

    def backward(carried, inputs):
        adjoint_real, adjoint_imag = carried
        mixed_rows, back_block = inputs
        gated, pullback = jax.vjp(jax.nn.gelu, mixed_rows)
        (interior_gradient,) = pullback(back_block)
        pulled_real_part = jnp.einsum(
            "woy,wom->wym", readout_real_part, interior_gradient, precision=finest_precision
        )[:, :, ::-1]
        pulled_imaginary = -jnp.einsum(
            "woy,wom->wym", readout_imaginary, interior_gradient, precision=finest_precision
        )[:, :, ::-1]
        pulled_real_part = pulled_real_part.at[:, :, 0].add(
            decay_real * adjoint_real + decay_imag * adjoint_imag
        )
        pulled_imaginary = pulled_imaginary.at[:, :, 0].add(
            decay_real * adjoint_imag - decay_imag * adjoint_real
        )
        _, _, running_real_part, running_imaginary = lax.associative_scan(
            combine, (factor_real, -factor_imag, pulled_real_part, pulled_imaginary), axis=2
        )
        running_real_part = running_real_part[:, :, ::-1]
        running_imaginary = running_imaginary[:, :, ::-1]
        grad_block = (
            jnp.einsum("gpc,gpk->gck", input_real, running_real_part, precision=finest_precision)
            + jnp.einsum("gpc,gpk->gck", input_imag, running_imaginary, precision=finest_precision)
            + skip_gain[:, :, None] * interior_gradient
        )
        return (
            (running_real_part[:, :, 0], running_imaginary[:, :, 0]),
            (grad_block.astype(jnp.bfloat16), gated.astype(jnp.bfloat16)),
        )

    _, (grad_blocks, gated_blocks) = lax.scan(
        backward, (empty_state, empty_state), (mixed_blocks, to_blocks(head_back)), reverse=True
    )

    def from_blocks(stacked):
        return jnp.moveaxis(stacked, 0, 2).reshape(own_width, length)

    return (from_blocks(grad_blocks), from_blocks(gated_blocks))


def on_device(
    tokens,
    cotangent,
    in_weight,
    out_weight,
    decay_rate,
    frequency,
    step_log,
    drive_real,
    drive_imag,
    readout_real_part,
    readout_imaginary,
    skip_gain,
):
    full_in, full_out = (
        lax.all_gather(in_weight, "sp", axis=0, tiled=True),
        lax.all_gather(out_weight, "sp", axis=0, tiled=True),
    )
    part_drive = jnp.einsum(
        "cd,td->ct", full_in, tokens, preferred_element_type=jnp.float32
    ).astype(jnp.bfloat16)
    part_back = jnp.einsum(
        "cd,td->ct", full_out, cotangent, preferred_element_type=jnp.float32
    ).astype(jnp.bfloat16)
    channels = part_drive.shape[0]
    rows_here = tokens.shape[0]
    seq_devices = lax.axis_size("sp")
    own_width = channels // seq_devices
    params = (
        decay_rate,
        frequency,
        step_log,
        drive_real,
        drive_imag,
        readout_real_part,
        readout_imaginary,
        skip_gain,
    )
    row_groups = lax.axis_size("dp")
    portion = rows_here // row_groups
    own_slot = lax.axis_index("dp") * portion
    drive_share, back_share = (
        lax.psum_scatter(part_drive, "dp", scatter_dimension=1, tiled=True).astype(jnp.float32),
        lax.psum_scatter(part_back, "dp", scatter_dimension=1, tiled=True).astype(jnp.float32),
    )
    drive_slice = drive_share.astype(jnp.bfloat16)[:, None, :]
    back_slice = back_share.astype(jnp.bfloat16)[:, None, :]
    drive_parts, back_parts = (
        lax.all_to_all(drive_slice, "sp", split_axis=0, concat_axis=1, tiled=True),
        lax.all_to_all(back_slice, "sp", split_axis=0, concat_axis=1, tiled=True),
    )
    drive_joined, back_joined = (
        lax.all_gather(drive_parts, "dp", axis=2, tiled=True),
        lax.all_gather(back_parts, "dp", axis=2, tiled=True),
    )
    head_grad, head_gated = mechanism(
        drive_joined.reshape(own_width, seq_devices * rows_here),
        back_joined.reshape(own_width, seq_devices * rows_here),
        params,
    )
    grad_slice = lax.dynamic_slice_in_dim(
        head_grad.reshape(own_width, seq_devices, rows_here), own_slot, portion, 2
    )
    gated_slice = lax.dynamic_slice_in_dim(
        head_gated.reshape(own_width, seq_devices, rows_here), own_slot, portion, 2
    )
    grad_parts, gated_parts = (
        lax.all_to_all(grad_slice, "sp", split_axis=1, concat_axis=0, tiled=True),
        lax.all_to_all(gated_slice, "sp", split_axis=1, concat_axis=0, tiled=True),
    )
    grad_joined, gated_joined = (
        lax.all_gather(grad_parts, "dp", axis=2, tiled=True),
        lax.all_gather(gated_parts, "dp", axis=2, tiled=True),
    )
    grad_cols = grad_joined.reshape(channels, rows_here)
    gated_cols = gated_joined.reshape(channels, rows_here)
    grad_tokens = jnp.einsum(
        "ct,cd->td", grad_cols, full_in, preferred_element_type=jnp.float32
    ).astype(jnp.bfloat16)
    grad_scale = (rows_here * seq_devices) ** (-0.5)
    picked = grad_cols
    grad_in_weight = lax.psum_scatter(
        jnp.einsum("ct,td->cd", picked, tokens, preferred_element_type=jnp.float32) * grad_scale,
        "sp",
        scatter_dimension=0,
        tiled=True,
    )
    picked = gated_cols
    grad_out_weight = lax.psum_scatter(
        jnp.einsum("ct,td->cd", picked, cotangent, preferred_element_type=jnp.float32) * grad_scale,
        "sp",
        scatter_dimension=0,
        tiled=True,
    )
    return (grad_tokens, grad_in_weight, grad_out_weight)


def solution(mesh):
    return jax.shard_map(
        on_device,
        mesh=mesh,
        in_specs=(
            P("sp", "dp"),
            P("sp", "dp"),
            P("sp", "dp"),
            P("sp", "dp"),
            P("sp", None),
            P("sp", None),
            P("sp"),
            P("sp", None, None),
            P("sp", None, None),
            P("sp", None, None),
            P("sp", None, None),
            P("sp", None),
        ),
        out_specs=(P("sp", "dp"), P("sp", "dp"), P("sp", "dp")),
        check_vma=False,
    )
```

profile of v0, /device:TPU:0, one launch (start us, length us, event | category | flops | bytes accessed | tf_op | source)
XLA Modules:
  0.0 653.4 jit_solution(1180258322243700626)
XLA Ops:
  7.2 45.7 %all_gather.20 = bf16[256,1024]{1,0:T(8,128)(2,1)S(1)} all-gather(bf16[16,1024]{1,0:T(8,128)(2,1)} %param.26), channel_id=1, replica_groups=mesh['sp'=16,'dp'=2] {'sp'}, dimensions={0}, use_global_device_ids=true | all-gather | bytes 557056 | tf_op jit(solution)/shard_map/all_gather | solution.py:140
  54.6 38.5 %all_gather.18 = bf16[256,1024]{1,0:T(8,128)(2,1)S(1)} all-gather(bf16[16,1024]{1,0:T(8,128)(2,1)S(1)} %copy-done.4), channel_id=1, replica_groups=mesh['sp'=16,'dp'=2] {'sp'}, dimensions={0}, use_global_device_ids=true | all-gather | bytes 557056 | tf_op jit(solution)/shard_map/all_gather | solution.py:141
  96.9 1.4 reduce.23
  99.1 3.5 all-to-all-start.1
  103.0 1.4 reduce.22
  105.2 4.8 all-to-all-done.1
  110.0 3.5 all-to-all-start
  114.0 2.2 all-gather.1
  118.6 164.4 %while.40 = (s32[]{:T(128)}, f32[1,32]{1,0:T(1,128)S(1)}, f32[1,32]{1,0:T(1,128)S(1)}, f32[4,1,16,512]{3,2,1,0:T(8,128)S(1)}, f32[4,1,16,512]{3,0,2,1:T(4,128)S(...) while((s32[]{:T(128)}, f32[1,32]{1,0:T(1,128)S(1)}, ...), condition=%wide.region_2.3_spmd, body=%wide.region_1.0_spmd.sunk | while | flops 12997378 | bytes 4572589 | solution.py:81
  120.7 1.1 slice.2926
  123.1 1.1 slice.2925
  124.2 1.1 slice.2922
  125.4 1.1 slice.2924
  151.0 1.1 slice.2994
  152.1 1.1 slice.2995
  153.2 1.1 slice.2996
  161.7 1.1 slice.2926
  164.1 1.1 slice.2925
  165.3 1.1 slice.2922
  166.4 1.1 slice.2924
  192.0 1.1 slice.2994
  193.2 1.1 slice.2995
  194.3 1.1 slice.2996
  202.8 1.1 slice.2926
  205.2 1.1 slice.2925
  206.3 1.1 slice.2922
  207.5 1.1 slice.2924
  233.1 1.1 slice.2994
  234.2 1.1 slice.2995
  235.4 1.1 slice.2996
  243.8 1.1 slice.2926
  246.3 1.1 slice.2925
  247.4 1.1 slice.2922
  248.5 1.1 slice.2924
  283.4 2.2 all-gather
  287.3 188.4 %while.41 = (s32[]{:T(128)}, f32[1,32]{1,0:T(1,128)S(1)}, f32[1,32]{1,0:T(1,128)S(1)}, bf16[4,1,16,512]{3,2,1,0:T(8,128)(2,1)S(1)}, bf16[4,1,16,512]{3,2,1,0:T(8...) while((s32[]{:T(128)}, f32[1,32]{1,0:T(1,128)S(1)}, ...), condition=%wide.region_5.6_spmd, body=%wide.region_4.0_spmd.sunk | while | flops 13562627 | bytes 5699549 | solution.py:115
  307.7 1.1 slice.3051
  310.2 1.1 slice.3050
  311.3 1.1 slice.3047
  312.5 1.1 slice.3049
  344.3 1.1 pad.1013
  350.4 1.1 slice.3051
  352.8 1.1 slice.3050
  354.0 1.1 slice.3047
  355.1 1.1 slice.3049
  387.0 1.1 pad.1013
  393.1 1.1 slice.3051
  395.5 1.1 slice.3050
  396.7 1.1 slice.3047
  397.8 1.1 slice.3049
  429.6 1.1 pad.1013
  435.7 1.1 slice.3051
  438.2 1.1 slice.3050
  439.3 1.1 slice.3047
  440.5 1.1 slice.3049
  472.3 1.1 pad.1013
  476.2 14.1 %all_to_all.72 = bf16[16,2,512]{2,1,0:T(2,128)(2,1)S(1)} all-to-all(bf16[16,2,512]{2,1,0:T(2,128)(2,1)S(1)} %reshape.604), channel_id=1, replica_groups=mesh['sp'=16,'dp'=2] {'sp'}, dimensions={0} | all-to-all | bytes 65536 | tf_op jit(solution)/shard_map/all_to_all | solution.py:193
  490.4 1.9 all_gather.23
  492.3 1.3 convolution_multiply_fusion
  493.8 10.1 %all_to_all.73 = bf16[16,2,512]{2,1,0:T(2,128)(2,1)S(1)} all-to-all(bf16[16,2,512]{2,1,0:T(2,128)(2,1)S(1)} %reshape.602), channel_id=1, replica_groups=mesh['sp'=16,'dp'=2] {'sp'}, dimensions={0} | all-to-all | bytes 65536 | tf_op jit(solution)/shard_map/all_to_all | solution.py:192
  504.1 1.9 all_gather.22
  506.0 1.3 convolution_multiply_fusion.1
  508.2 60.7 %reduce-scatter.11.cloned.1.call-done = f32[16,1024]{1,0:T(8,128)} async-done(((f32[256,1024]{1,0:T(8,128)}), f32[16,1024]{1,0:T(8,128)}) %reduce-scatter.11.cloned.1.call-update) | async-done | bytes 65552 | tf_op jit(solution)/shard_map/reduce_scatter | solution.py:213
  568.9 77.7 %reduce-scatter.9.cloned.1.call-done = f32[16,1024]{1,0:T(8,128)} async-done(((f32[256,1024]{1,0:T(8,128)}), f32[16,1024]{1,0:T(8,128)}) %reduce-scatter.9.cloned.1.call-update) | async-done | bytes 65552 | tf_op jit(solution)/shard_map/reduce_scatter | solution.py:206
  (1468 shorter events, 289.6 us)
Async XLA Ops:
  7.2 86.0 %copy-start = (bf16[128,1024]{1,0:T(8,128)(2,1)S(1)}, bf16[128,1024]{1,0:T(8,128)(2,1)}, u32[]{:S(2)}) copy-start(bf16[128,1024]{1,0:T(8,128)(2,1)} %param.25) | copy-start | bytes 786436
  7.2 45.7 %copy-start.1 = (bf16[128,1024]{1,0:T(8,128)(2,1)S(1)}, bf16[128,1024]{1,0:T(8,128)(2,1)}, u32[]{:S(2)}) copy-start(bf16[128,1024]{1,0:T(8,128)(2,1)} %param.24) | copy-start | bytes 786436
  7.2 89.1 %reduce-scatter.7.cloned.1.call-start = ((), (), s32[]{:S(2)}) async-start(), calls=%async_computation.9 | async-start | bytes 98304 | tf_op jit(solution)/shard_map/reduce_scatter | solution.py:167
  53.9 0.8 copy-start.4
  53.9 49.1 %reduce-scatter.5.cloned.1.call-start = ((), (), s32[]{:S(2)}) async-start(), calls=%async_computation.8 | async-start | bytes 98304 | tf_op jit(solution)/shard_map/reduce_scatter | solution.py:168
  94.8 0.7 copy-start.8
  94.9 0.7 copy-start.9
  95.6 0.7 copy-start.6
  95.6 0.7 copy-start.7
  99.1 10.9 %all-to-all-start.1 = ((bf16[16,2,512]{2,1,0:T(2,128)(2,1)}), bf16[16,2,512]{2,1,0:T(2,128)(2,1)S(1)}, u32[]{:S(2)}, u32[]{:S(2)}) async-start(bf16[16,2,512]{2,1,0:T(2,128)(2,1)} %reshape.600), calls=%async_computation.3 | async-start | bytes 65536 | tf_op jit(solution)/shard_map/all_to_all | solution.py:173
  110.0 173.0 %all-to-all-start = ((bf16[16,2,512]{2,1,0:T(2,128)(2,1)}), bf16[16,2,512]{2,1,0:T(2,128)(2,1)S(1)}, u32[]{:S(2)}, u32[]{:S(2)}) async-start(bf16[16,2,512]{2,1,0:T(2,128)(2,1)} %reshape.598), calls=%async_computation.1 | async-start | bytes 65536 | tf_op jit(solution)/shard_map/all_to_all | solution.py:174
  113.5 455.4 %reduce-scatter.11.cloned.1.call-start = ((), (), s32[]{:S(2)}) async-start(), calls=%async_computation.11 | async-start | bytes 1114112 | tf_op jit(solution)/shard_map/reduce_scatter | solution.py:213
  117.8 0.7 copy-start.2
  117.8 0.7 copy-start.3
  117.9 0.7 copy-start.5
  493.6 153.0 %reduce-scatter.9.cloned.1.call-start = ((), (), s32[]{:S(2)}) async-start(), calls=%async_computation.10 | async-start | bytes 1114112 | tf_op jit(solution)/shard_map/reduce_scatter | solution.py:206
Sparse Core Ops, SparseCore 0:
  54.0 3.3 reduce-scatter.6
  94.3 5.1 reduce-scatter.4
  493.7 75.1 reduce-scatter.10
  571.6 75.0 reduce-scatter.8
where the time goes:
time: 657 us; the launch traced here: 653 us
  local copies, waits for them, and re-layouts  313 us (48%)
  waiting for transfers between devices  143 us (22%)
  blocking collectives  117 us (18%)
  loops' own time  25.5 us (4%)
  other arithmetic  20.8 us (3%)
  between operations  14.9 us (2%)
  matrix products  11.7 us (2%)
  starting transfers between devices  7.16 us (1%)
    slice x328, local copies, waits for them, and re-layouts, forward(): lax.associative_scan(combine, (factor_real, factor_imag, push_real, push_...  106 us
    slice x327, local copies, waits for them, and re-layouts, backward(): lax.associative_scan(combine, (factor_real, -factor_imag, pulled_real_par...  106 us
    reduce_scatter x1, waiting for transfers between devices, on_device(): lax.psum_scatter(jnp.einsum('ct,td->cd', picked, tokens, preferred_elemen...  77.7 us
    reduce_scatter x1, waiting for transfers between devices, on_device(): lax.psum_scatter(jnp.einsum('ct,td->cd', picked, cotangent, preferred_ele...  60.7 us
    all_gather x1, blocking collectives, on_device(): lax.all_gather(in_weight, 'sp', axis=0, tiled=True)  45.7 us
    pad x128, local copies, waits for them, and re-layouts, backward(): lax.associative_scan(combine, (factor_real, -factor_imag, pulled_real_par...  41.8 us
    pad x128, local copies, waits for them, and re-layouts, forward(): lax.associative_scan(combine, (factor_real, factor_imag, push_real, push_...  41.8 us
    all_gather x1, blocking collectives, on_device(): lax.all_gather(out_weight, 'sp', axis=0, tiled=True)  38.5 us
  transfers between devices with their start and end apart: 6, of which 3 were waited for; matrix products, arithmetic and copies ran while one was open for 26% of the time, Pallas kernels for 0%

commit v1 on v0

--- a/solution.py
+++ b/solution.py
@@ -137,7 +137,9 @@
     skip_gain,
 ):
     full_in, full_out = (
-        lax.all_gather(in_weight, "sp", axis=0, tiled=True),
+        jnp.concatenate(
+            lax.all_to_all(jnp.stack([in_weight] * lax.axis_size("sp")), "sp", 0, 0), axis=0
+        ),
         lax.all_gather(out_weight, "sp", axis=0, tiled=True),
     )
     part_drive = jnp.einsum(

time: 657 us -> 644 us (0.980)
  blocking collectives: 117 us -> 74.2 us
  waiting for transfers between devices: 143 us -> 158 us
  starting transfers between devices: 7.16 us -> 22.1 us
    all_gather x1 -> x0, blocking collectives: 45.7 us -> none  [on_device(): lax.all_gather(in_weight, 'sp', axis=0, tiled=True)]
    reduce_scatter x1, waiting for transfers between devices: 0.01 us -> 11.4 us  [on_device(): lax.psum_scatter(part_drive, 'dp', scatter_dimension=1, tiled=True)]
    all_to_all x0 -> x1, starting transfers between devices: none -> 8.47 us  [on_device(): lax.all_to_all(jnp.stack([in_weight] * lax.axis_size('sp')), 'sp', 0, 0)]
    all_gather x1, blocking collectives: 38.5 us -> 45.8 us  [on_device(): lax.all_gather(out_weight, 'sp', axis=0, tiled=True)]
  transfers between devices with their start and end apart: 6 -> 7, of which waited for: 3 -> 5; matrix products, arithmetic and copies ran while one was open for 26% -> 2% of each run, Pallas kernels for 0% -> 0%
where the time goes in v1:
time: 644 us; the launch traced here: 640 us
  local copies, waits for them, and re-layouts  313 us (49%)
  waiting for transfers between devices  158 us (25%)
  blocking collectives  74.2 us (12%)
  loops' own time  25.5 us (4%)
  starting transfers between devices  22.1 us (3%)
  other arithmetic  20.9 us (3%)
  between operations  15 us (2%)
  matrix products  11.8 us (2%)
    slice x328, local copies, waits for them, and re-layouts, forward(): lax.associative_scan(combine, (factor_real, factor_imag, push_real, push_...  106 us
    slice x327, local copies, waits for them, and re-layouts, backward(): lax.associative_scan(combine, (factor_real, -factor_imag, pulled_real_par...  106 us
    reduce_scatter x1, waiting for transfers between devices, on_device(): lax.psum_scatter(jnp.einsum('ct,td->cd', picked, tokens, preferred_elemen...  77.7 us
    reduce_scatter x1, waiting for transfers between devices, on_device(): lax.psum_scatter(jnp.einsum('ct,td->cd', picked, cotangent, preferred_ele...  60.7 us
    all_gather x1, blocking collectives, on_device(): lax.all_gather(out_weight, 'sp', axis=0, tiled=True)  45.8 us
    pad x128, local copies, waits for them, and re-layouts, backward(): lax.associative_scan(combine, (factor_real, -factor_imag, pulled_real_par...  41.8 us
    pad x128, local copies, waits for them, and re-layouts, forward(): lax.associative_scan(combine, (factor_real, factor_imag, push_real, push_...  41.8 us
    another operation x1, loops' own time, mechanism(): lax.scan(backward, (empty_state, empty_state), (mixed_blocks, to_blocks(h...  21.6 us
  transfers between devices with their start and end apart: 7, of which 5 were waited for; matrix products, arithmetic and copies ran while one was open for 2% of the time, Pallas kernels for 0%

profile of v1, /device:TPU:0, one launch (start us, length us, event | category | flops | bytes accessed | tf_op | source)
XLA Modules:
  0.0 640.4 jit_solution(13633234733847197750)
XLA Ops:
  7.2 1.7 stack.2
  8.8 8.5 %all-to-all-start.1 = ((bf16[16,16,1024]{2,1,0:T(8,128)(2,1)}), bf16[16,16,1024]{2,1,0:T(8,128)(2,1)S(1)}, u32[]{:S(2)}, u32[]{:S(2)}) async-start(bf16[16,16,1024]{2,1,0:T(8,128)(2,1)} %stack.2), calls=%async_computation.2 | async-start | bytes 1048576 | tf_op jit(solution)/shard_map/all_to_all | solution.py:141
  17.4 45.8 %all_gather.15 = bf16[256,1024]{1,0:T(8,128)(2,1)S(1)} all-gather(bf16[16,1024]{1,0:T(8,128)(2,1)S(1)} %copy-done.4), channel_id=1, replica_groups=mesh['sp'=16,'dp'=2] {'sp'}, dimensions={0}, use_global_device_ids=true | all-gather | bytes 557056 | tf_op jit(solution)/shard_map/all_gather | solution.py:143
  65.1 4.2 reduce-scatter.5.cloned.1.call-done
  69.8 1.4 reduce.22
  72.0 6.7 %all-to-all-start = ((bf16[16,2,512]{2,1,0:T(2,128)(2,1)}), bf16[16,2,512]{2,1,0:T(2,128)(2,1)S(1)}, u32[]{:S(2)}, u32[]{:S(2)}) async-start(bf16[16,2,512]{2,1,0:T(2,128)(2,1)} %reshape.604), calls=%async_computation.1 | async-start | bytes 65536 | tf_op jit(solution)/shard_map/all_to_all | solution.py:176
  79.8 11.4 %reduce-scatter.7.cloned.1.call-done = bf16[256,64]{0,1:T(8,128)(2,1)} async-done(((bf16[256,128]{0,1:T(8,128)(2,1)}), bf16[256,64]{0,1:T(8,128)(2,1)}) %reduce-scatter.7.cloned.1.call-update) | async-done | bytes 32784 | tf_op jit(solution)/shard_map/reduce_scatter | solution.py:169
  91.2 1.4 reduce.23
  93.5 6.7 %all-to-all-start.2 = ((bf16[16,2,512]{2,1,0:T(2,128)(2,1)}), bf16[16,2,512]{2,1,0:T(2,128)(2,1)S(1)}, u32[]{:S(2)}, u32[]{:S(2)}) async-start(bf16[16,2,512]{2,1,0:T(2,128)(2,1)} %reshape.606), calls=%async_computation.4 | async-start | bytes 65536 | tf_op jit(solution)/shard_map/all_to_all | solution.py:175
  101.0 2.2 all-gather
  103.7 3.9 all-to-all-done.2
  108.0 2.2 all-gather.1
  112.7 164.4 %while.40 = (s32[]{:T(128)}, f32[1,32]{1,0:T(1,128)S(1)}, f32[1,32]{1,0:T(1,128)S(1)}, f32[4,1,16,512]{3,2,1,0:T(8,128)S(1)}, f32[4,1,16,512]{3,0,2,1:T(4,128)S(...) while((s32[]{:T(128)}, f32[1,32]{1,0:T(1,128)S(1)}, ...), condition=%wide.region_2.3_spmd, body=%wide.region_1.0_spmd.sunk | while | flops 12997378 | bytes 4572589 | solution.py:81
  114.7 1.1 slice.2926
  117.1 1.1 slice.2925
  118.3 1.1 slice.2922
  119.4 1.1 slice.2924
  146.2 1.1 slice.2995
  147.3 1.1 slice.2996
  155.8 1.1 slice.2926
  158.2 1.1 slice.2925
  159.3 1.1 slice.2922
  160.5 1.1 slice.2924
  187.2 1.1 slice.2995
  188.4 1.1 slice.2996
  196.8 1.1 slice.2926
  199.2 1.1 slice.2925
  200.4 1.1 slice.2922
  201.5 1.1 slice.2924
  227.1 1.1 slice.2994
  229.4 1.1 slice.2996
  237.9 1.1 slice.2926
  240.3 1.1 slice.2925
  241.5 1.1 slice.2922
  242.6 1.1 slice.2924
  278.3 188.4 %while.41 = (s32[]{:T(128)}, f32[1,32]{1,0:T(1,128)S(1)}, f32[1,32]{1,0:T(1,128)S(1)}, bf16[4,1,16,512]{3,2,1,0:T(8,128)(2,1)S(1)}, bf16[4,1,16,512]{3,2,1,0:T(8...) while((s32[]{:T(128)}, f32[1,32]{1,0:T(1,128)S(1)}, ...), condition=%wide.region_5.6_spmd, body=%wide.region_4.0_spmd.sunk | while | flops 13562627 | bytes 5699549 | solution.py:115
  298.7 1.1 slice.3051
  301.2 1.1 slice.3050
  302.3 1.1 slice.3047
  303.4 1.1 slice.3049
  335.3 1.1 pad.1013
  341.4 1.1 slice.3051
  343.8 1.1 slice.3050
  345.0 1.1 slice.3047
  346.1 1.1 slice.3049
  377.9 1.1 pad.1013
  384.0 1.1 slice.3051
  386.5 1.1 slice.3050
  387.6 1.1 slice.3047
  388.8 1.1 slice.3049
  420.6 1.1 pad.1013
  426.7 1.1 slice.3051
  429.2 1.1 slice.3050
  430.3 1.1 slice.3047
  431.4 1.1 slice.3049
  463.3 1.1 pad.1013
  467.1 10.2 %all_to_all.77 = bf16[16,2,512]{2,1,0:T(2,128)(2,1)S(1)} all-to-all(bf16[16,2,512]{2,1,0:T(2,128)(2,1)S(1)} %reshape.610), channel_id=1, replica_groups=mesh['sp'=16,'dp'=2] {'sp'}, dimensions={0} | all-to-all | bytes 65536 | tf_op jit(solution)/shard_map/all_to_all | solution.py:195
  477.5 1.9 all_gather.19
  479.4 1.3 convolution_multiply_fusion
  480.9 10.1 %all_to_all.78 = bf16[16,2,512]{2,1,0:T(2,128)(2,1)S(1)} all-to-all(bf16[16,2,512]{2,1,0:T(2,128)(2,1)S(1)} %reshape.608), channel_id=1, replica_groups=mesh['sp'=16,'dp'=2] {'sp'}, dimensions={0} | all-to-all | bytes 65536 | tf_op jit(solution)/shard_map/all_to_all | solution.py:194
  491.2 1.9 all_gather.18
  493.1 1.3 convolution_multiply_fusion.1
  495.3 60.7 %reduce-scatter.11.cloned.1.call-done = f32[16,1024]{1,0:T(8,128)} async-done(((f32[256,1024]{1,0:T(8,128)}), f32[16,1024]{1,0:T(8,128)}) %reduce-scatter.11.cloned.1.call-update) | async-done | bytes 65552 | tf_op jit(solution)/shard_map/reduce_scatter | solution.py:215
  556.0 77.7 %reduce-scatter.9.cloned.1.call-done = f32[16,1024]{1,0:T(8,128)} async-done(((f32[256,1024]{1,0:T(8,128)}), f32[16,1024]{1,0:T(8,128)}) %reduce-scatter.9.cloned.1.call-update) | async-done | bytes 65552 | tf_op jit(solution)/shard_map/reduce_scatter | solution.py:208
  (1470 shorter events, 291.0 us)
Async XLA Ops:
  7.2 56.0 %copy-start = (bf16[128,1024]{1,0:T(8,128)(2,1)S(1)}, bf16[128,1024]{1,0:T(8,128)(2,1)}, u32[]{:S(2)}) copy-start(bf16[128,1024]{1,0:T(8,128)(2,1)} %param.25) | copy-start | bytes 786436
  8.8 8.5 %copy-start.4 = (bf16[16,1024]{1,0:T(8,128)(2,1)S(1)}, bf16[16,1024]{1,0:T(8,128)(2,1)}, u32[]{:S(2)}) copy-start(bf16[16,1024]{1,0:T(8,128)(2,1)} %param.27) | copy-start | bytes 98308
  8.8 63.2 %all-to-all-start.1 = ((bf16[16,16,1024]{2,1,0:T(8,128)(2,1)}), bf16[16,16,1024]{2,1,0:T(8,128)(2,1)S(1)}, u32[]{:S(2)}, u32[]{:S(2)}) async-start(bf16[16,16,1024]{2,1,0:T(8,128)(2,1)} %stack.2), calls=%async_computation.2 | async-start | bytes 1048576 | tf_op jit(solution)/shard_map/all_to_all | solution.py:141
  17.3 51.9 %reduce-scatter.5.cloned.1.call-start = ((), (), s32[]{:S(2)}) async-start(), calls=%async_computation.9 | async-start | bytes 98304 | tf_op jit(solution)/shard_map/reduce_scatter | solution.py:170
  63.2 1.7 copy-start.8
  63.2 1.7 copy-start.9
  63.2 1.8 copy-start.6
  63.2 1.8 copy-start.7
  64.2 14.7 %copy-start.1 = (bf16[128,1024]{1,0:T(8,128)(2,1)S(1)}, bf16[128,1024]{1,0:T(8,128)(2,1)}, u32[]{:S(2)}) copy-start(bf16[128,1024]{1,0:T(8,128)(2,1)} %param.24) | copy-start | bytes 786436
  72.0 21.5 %all-to-all-start = ((bf16[16,2,512]{2,1,0:T(2,128)(2,1)}), bf16[16,2,512]{2,1,0:T(2,128)(2,1)S(1)}, u32[]{:S(2)}, u32[]{:S(2)}) async-start(bf16[16,2,512]{2,1,0:T(2,128)(2,1)} %reshape.604), calls=%async_computation.1 | async-start | bytes 65536 | tf_op jit(solution)/shard_map/all_to_all | solution.py:176
  78.8 12.4 %reduce-scatter.7.cloned.1.call-start = ((), (), s32[]{:S(2)}) async-start(), calls=%async_computation.10 | async-start | bytes 98304 | tf_op jit(solution)/shard_map/reduce_scatter | solution.py:169
  93.5 14.1 %all-to-all-start.2 = ((bf16[16,2,512]{2,1,0:T(2,128)(2,1)}), bf16[16,2,512]{2,1,0:T(2,128)(2,1)S(1)}, u32[]{:S(2)}, u32[]{:S(2)}) async-start(bf16[16,2,512]{2,1,0:T(2,128)(2,1)} %reshape.606), calls=%async_computation.4 | async-start | bytes 65536 | tf_op jit(solution)/shard_map/all_to_all | solution.py:175
  100.2 455.8 %reduce-scatter.11.cloned.1.call-start = ((), (), s32[]{:S(2)}) async-start(), calls=%async_computation.12 | async-start | bytes 1114112 | tf_op jit(solution)/shard_map/reduce_scatter | solution.py:215
  111.9 0.7 copy-start.2
  111.9 0.7 copy-start.3
  112.0 0.7 copy-start.5
  480.7 152.9 %reduce-scatter.9.cloned.1.call-start = ((), (), s32[]{:S(2)}) async-start(), calls=%async_computation.11 | async-start | bytes 1114112 | tf_op jit(solution)/shard_map/reduce_scatter | solution.py:208
Sparse Core Ops, SparseCore 0:
  64.3 4.8 reduce-scatter.4
  82.3 8.8 reduce-scatter.6
  480.8 75.1 reduce-scatter.10
  558.7 74.9 reduce-scatter.8
